TPU v7x, 32 devices: a whole 2x2x4 slice. The times are simulated.
32 devices in a mesh: kv: 8 (over z, x), tp: 4 (over y, core).
Axes of the slice: x: 2, y: 2, z: 4, core: 2. Of those that a mesh axis runs over, the one named last changes fastest.
Arguments:
- tokens: bfloat16 [16, 4096], P(None, 'kv'), may hold values from -400 to 400
- norm_gain: bfloat16 [4096], P('kv'), may hold values from 0.099609375 to 1.8984375
- query_weight: bfloat16 [4096, 4096], P('kv', 'tp'), may hold values from -0.09375 to 0.09375
- key_weight: bfloat16 [4096, 4096], P('kv', 'tp'), may hold values from -0.5 to 0.5
- value_weight: bfloat16 [4096, 4096], P('kv', 'tp'), may hold values from -0.09375 to 0.09375
- out_weight: bfloat16 [4096, 4096], P('tp', 'kv'), may hold values from -0.09375 to 0.09375
- diff_scale: float32 [32], P('tp'), may hold values from 0.3 to 0.8
- head_gain: float32 [128], replicated, may hold values from 0.1 to 1.9
- key_cache: bfloat16 [1, 1024, 32, 128], P(None, 'kv', 'tp'), may hold values from -96 to 96
- value_cache: bfloat16 [1, 1024, 32, 128], P(None, 'kv', 'tp'), may hold values from -6 to 6
- cache_filled: int32 [1], replicated, may hold values from 512 to 992
- accepted: int32 [1], replicated, may hold values from 0 to 16
- parents: int32 [1, 16], replicated, may hold values from -1 to 14, as said below
Outputs:
- mixed: bfloat16 [16, 4096], P(None, 'kv')
- key_cache_new: bfloat16 [1, 1024, 32, 128], P(None, 'kv', 'tp')
- value_cache_new: bfloat16 [1, 1024, 32, 128], P(None, 'kv', 'tp')
Inputs may be any that keep to these rules, and one draw needn't show every extreme that they name: `parents`: the parent of proposal j is -1 or an earlier proposal of the same sequence; proposal 0's parent is -1; the last proposal's parent is the proposal before it.
All inputs are finite; a program needn't handle non-finite values.
Results may differ from a plain program's by a relative error of at most 0.015.
Values may be sent and summed in bfloat16 or wider, within the bound.
A program may use at most 64 MiB of HBM per device.

v0:
```python
import functools

import jax
import jax.numpy as jnp
from jax import lax
from jax.experimental import pallas as pl
from jax.experimental.pallas import tpu as pltpu
from jax.sharding import PartitionSpec as P

D = 4096
DH = 64
DV = 128


def joined(value, axis, join):
    pieces = jax.tree.map(lambda part: lax.all_gather(part, axis), value)
    head = jax.tree.map(lambda part: part[0], pieces)
    tail = jax.tree.map(lambda part: part[1:], pieces)
    so_far, _ = lax.scan(lambda so_far, share: (join(so_far, share), None), head, tail)
    return so_far


def ancestry(parents):
    count = parents.shape[1]
    links = (parents[:, :, None] == jnp.arange(count, dtype=jnp.int32)[None, None, :]).astype(
        jnp.float32
    )
    identity = jnp.eye(count, dtype=jnp.float32)
    reach = jnp.minimum(identity[None] + links, 1.0)
    for turn in range(count.bit_length()):
        reach = jnp.minimum(jnp.einsum("spj,sjk->spk", reach, reach), 1.0)
    return reach > 0.5


def combine(earlier, later):
    highest = jnp.maximum(earlier[0], later[0])
    factor_one = jnp.exp(earlier[0] - highest)
    factor_two = jnp.exp(later[0] - highest)
    total = earlier[1] * factor_one + later[1] * factor_two
    values_sum = earlier[2] * factor_one[..., None] + later[2] * factor_two[..., None]
    return (highest, total, values_sum)


def head_norm(head_out, head_gain):
    return (
        head_out
        * lax.rsqrt(jnp.mean(head_out * head_out, axis=-1, keepdims=True) + 1e-05)
        * head_gain
    )


def shards(
    tokens,
    norm_gain,
    query_weight,
    key_weight,
    value_weight,
    out_weight,
    diff_scale,
    head_gain,
    key_cache,
    value_cache,
    cache_filled,
    accepted,
    parents,
):
    seq_count = key_cache.shape[0]
    span = key_cache.shape[1]
    heads_here = key_cache.shape[2]
    proposals = tokens.shape[0] // seq_count
    inv_root = DH ** (-0.5)
    xfloat = tokens.astype(jnp.float32)
    squares = jnp.sum(xfloat * xfloat, axis=1)
    normed = (xfloat * norm_gain.astype(jnp.float32)).astype(jnp.bfloat16)
    partial_value = jnp.concatenate(
        [
            jnp.dot(normed, query_weight, preferred_element_type=jnp.float32),
            jnp.dot(normed, key_weight, preferred_element_type=jnp.float32),
            jnp.dot(normed, value_weight, preferred_element_type=jnp.float32),
        ],
        axis=1,
    )
    totals, square_sum = lax.psum((partial_value, squares), "kv")
    row_scale = lax.rsqrt(square_sum / D + 1e-06)
    projected = (totals * row_scale[:, None]).astype(jnp.bfloat16)
    q_width = heads_here * 2 * DH
    queries = projected[:, :q_width].reshape(seq_count, proposals, heads_here, 2, DH)
    fresh_k = projected[:, q_width : 2 * q_width].reshape(seq_count, proposals, heads_here * 2 * DH)
    fresh_v = projected[:, 2 * q_width :].reshape(seq_count, proposals, heads_here * DV)
    cached_k = key_cache.reshape(seq_count, span, heads_here, 2, DH)
    scores = (
        jnp.einsum("sphmd,schmd->shmpc", queries, cached_k, preferred_element_type=jnp.float32)
        * inv_root
    )
    places = lax.axis_index("kv") * span + jnp.arange(span, dtype=jnp.int32)
    valid_rows = cache_filled + accepted
    visible = (places[None, :] < valid_rows[:, None])[:, None, None, None, :]
    local_max = jnp.max(jnp.where(visible, scores, -1e30), axis=-1)
    weights = jnp.where(visible, jnp.exp(scores - local_max[..., None]), 0.0)
    sums = jnp.sum(weights, axis=-1)
    weighted = jnp.einsum(
        "shmpc,schd->shmpd",
        weights.astype(jnp.bfloat16),
        value_cache,
        preferred_element_type=jnp.float32,
    )
    reach = ancestry(parents)
    own_keys = fresh_k.reshape(seq_count, proposals, heads_here, 2, DH)
    own_scores = (
        jnp.einsum("sphmd,sjhmd->shmpj", queries, own_keys, preferred_element_type=jnp.float32)
        * inv_root
    )
    own_visible = reach[:, None, None]
    own_max = jnp.max(jnp.where(own_visible, own_scores, -1e30), axis=-1)
    own_weights = jnp.where(own_visible, jnp.exp(own_scores - own_max[..., None]), 0.0)
    own_sums = jnp.sum(own_weights, axis=-1)
    own_values = fresh_v.reshape(seq_count, proposals, heads_here, DV)
    own_weighted = jnp.einsum(
        "shmpj,sjhd->shmpd",
        own_weights.astype(jnp.bfloat16),
        own_values,
        preferred_element_type=jnp.float32,
    )
    highest, total, values_sum = combine(
        joined((local_max, sums, weighted), "kv", combine), (own_max, own_sums, own_weighted)
    )
    maps = values_sum / total[..., None]
    second_weight = diff_scale[None, :, None, None]
    head_out = maps[:, :, 0] - second_weight * maps[:, :, 1]
    head_out = head_norm(jnp.transpose(head_out, (0, 2, 1, 3)), head_gain)
    flat = head_out.astype(jnp.bfloat16).reshape(seq_count * proposals, heads_here * DV)
    partial_out = jnp.dot(flat, out_weight, preferred_element_type=jnp.float32)
    mixed = lax.psum(partial_out.astype(jnp.bfloat16), "tp")
    relative = places[None, :] - valid_rows[:, None]
    one_hot = (
        relative[:, :, None] == jnp.arange(proposals, dtype=jnp.int32)[None, None, :]
    ).astype(jnp.bfloat16)
    inside = ((relative >= 0) & (relative < proposals))[:, :, None]
    placed_k = jnp.einsum(
        "scj,sjx->scx", one_hot, fresh_k, preferred_element_type=jnp.float32
    ).astype(jnp.bfloat16)
    placed_v = jnp.einsum(
        "scj,sjx->scx", one_hot, fresh_v, preferred_element_type=jnp.float32
    ).astype(jnp.bfloat16)
    key_out = jnp.where(
        inside, placed_k, key_cache.reshape(seq_count, span, heads_here * 2 * DH)
    ).reshape(key_cache.shape)
    value_out = jnp.where(
        inside, placed_v, value_cache.reshape(seq_count, span, heads_here * DV)
    ).reshape(value_cache.shape)
    return (mixed, key_out, value_out)


MESH = pl.DeviceIdType.MESH
BF = jnp.bfloat16
F32 = jnp.float32
PART = jnp.float32
UTYPE = jnp.bfloat16
VMEM_BYTES = 67043328


def dot(a, b):
    return jnp.dot(a, b, preferred_element_type=F32)


def iota(shape, dim):
    return lax.broadcasted_iota(jnp.int32, shape, dim)


def kernel(
    n,
    n_tp,
    heads,
    tok_hbm,
    gain_hbm,
    hgain_hbm,
    wq_hbm,
    wk_hbm,
    wv_hbm,
    wo_hbm,
    kc_hbm,
    vc_hbm,
    scale_ref,
    filled_ref,
    accepted_ref,
    parents_ref,
    mixed_ref,
    ko,
    vo,
    tok_ref,
    gain_ref,
    hgain_ref,
    wq,
    wk,
    wv,
    wo,
    kc,
    vc,
    kf,
    vf,
    kh,
    vh,
    sq_send,
    sq_recv,
    q_send,
    q_recv,
    kv_send,
    kv_recv,
    qg_send,
    qg_recv,
    kvg_send,
    kvg_recv,
    u_send,
    u_recv,
    ms_send,
    ms_recv,
    hg_send,
    hg_recv,
    m_send,
    m_recv,
    local_sem,
    send_sem,
    recv_sem,
    tsend_sem,
    trecv_sem,
):
    me = lax.axis_index("kv")
    tp = lax.axis_index("tp")
    rows = tok_ref.shape[0]
    pair = 2 * rows
    loads = []
    for i, (src, dst) in enumerate(
        (
            (tok_hbm, tok_ref),
            (gain_hbm, gain_ref),
            (wq_hbm, wq),
            (wk_hbm, wk),
            (wv_hbm, wv),
            (kc_hbm, kc),
            (vc_hbm, vc),
            (hgain_hbm, hgain_ref),
            (wo_hbm, wo),
        )
    ):
        load = pltpu.make_async_copy(src, dst, local_sem.at[i])
        load.start()
        loads.append(load)
    peers = [lax.rem(me + off, n) for off in range(1, n)]
    tpeers = [lax.rem(tp + off, n_tp) for off in range(1, n_tp)]
    barrier = pltpu.get_barrier_semaphore()
    for peer in peers:
        pl.semaphore_signal(barrier, inc=1, device_id={"kv": peer}, device_id_type=MESH)
    for peer in tpeers:
        pl.semaphore_signal(barrier, inc=1, device_id={"tp": peer}, device_id_type=MESH)

    started = []

    def spread(phase, pick, recv):
        for peer in peers:
            copy = pltpu.make_async_remote_copy(
                src_ref=pick(peer),
                dst_ref=recv.at[me],
                send_sem=send_sem.at[phase, peer],
                recv_sem=recv_sem.at[phase, me],
                device_id={"kv": peer},
                device_id_type=MESH,
            )
            copy.start()
            started.append(copy)

    def arrive(phase, recv):
        for peer in peers:
            pltpu.make_async_remote_copy(
                src_ref=recv.at[peer],
                dst_ref=recv.at[peer],
                send_sem=send_sem.at[phase, peer],
                recv_sem=recv_sem.at[phase, peer],
                device_id={"kv": peer},
                device_id_type=MESH,
            ).wait_recv()

    loads[0].wait()
    loads[1].wait()
    xfloat = tok_ref[...].astype(F32)
    squares = jnp.sum(xfloat * xfloat, axis=1, keepdims=True)
    sq_send[...] = jnp.broadcast_to(squares, sq_send.shape)
    gain = gain_ref[...].astype(F32)
    gain = jnp.concatenate([gain[i : i + 1] for i in range(gain.shape[0])], axis=1)
    normed = (xfloat * gain).astype(BF)

    links = jnp.zeros((rows, rows), F32)
    sub, lane = iota((rows, rows), 0), iota((rows, rows), 1)
    for p in range(rows):
        links = jnp.where((sub == p) & (lane == parents_ref[0, p]), 1.0, links)
    reach = jnp.where(sub == lane, 1.0, links)
    for turn in range((rows - 1).bit_length()):
        reach = jnp.minimum(dot(reach.astype(BF), reach.astype(BF)), 1.0)

    loads[2].wait()
    part = dot(normed, wq[...])
    for h in range(heads):
        q_send[h] = part[:, h * DV : (h + 1) * DV].astype(PART)
    pl.semaphore_wait(barrier, (n - 1) + (n_tp - 1))
    spread(0, lambda peer: sq_send, sq_recv)
    spread(1, lambda peer: q_send.at[peer], q_recv)
    loads[3].wait()
    part = dot(normed, wk[...])
    for h in range(heads):
        kv_send[h, :rows] = part[:, h * DV : (h + 1) * DV].astype(PART)
    loads[4].wait()
    part = dot(normed, wv[...])
    for h in range(heads):
        kv_send[h, rows:] = part[:, h * DV : (h + 1) * DV].astype(PART)
    spread(2, lambda peer: kv_send.at[peer], kv_recv)

    count = kc.shape[0]
    span = count // heads
    loads[5].wait()
    loads[6].wait()
    loads[7].wait()
    for cache, wide, by_head in ((kc, kf, kh), (vc, vf, vh)):
        wide[...] = cache[...].astype(F32)
        for h in range(heads):
            by_head[h] = wide[pl.ds(h, span, stride=heads), :].astype(BF)

    sq_recv[me] = sq_send[...]
    q_recv[me] = q_send[me]
    arrive(0, sq_recv)
    total = sq_recv[0]
    for i in range(1, n):
        total = total + sq_recv[i]
    row_scale = lax.rsqrt(total / (n * tok_ref.shape[1]) + 1e-06)
    arrive(1, q_recv)
    q_sum = q_recv[0].astype(F32)
    for i in range(1, n):
        q_sum = q_sum + q_recv[i].astype(F32)
    query = (q_sum * row_scale).astype(BF)
    qg_send[...] = query
    spread(3, lambda peer: qg_send, qg_recv)
    qg_recv[me] = query

    kv_recv[me] = kv_send[me]
    arrive(2, kv_recv)
    kv_sum = kv_recv[0].astype(F32)
    for i in range(1, n):
        kv_sum = kv_sum + kv_recv[i].astype(F32)
    fresh_k = (kv_sum[:rows] * row_scale).astype(BF)
    fresh_v = (kv_sum[rows:] * row_scale).astype(BF)
    kvg_send[:rows] = fresh_k
    kvg_send[rows:] = fresh_v
    spread(4, lambda peer: kvg_send, kvg_recv)
    kvg_recv[me, :rows] = fresh_k
    kvg_recv[me, rows:] = fresh_v

    inv_root = DH ** (-0.5)
    first_map = iota((rows, DV), 1) < DH

    def two_maps(query):
        scaled = query.astype(F32) * inv_root
        one = jnp.where(first_map, scaled, 0.0).astype(BF)
        two = jnp.where(first_map, 0.0, scaled).astype(BF)
        return jnp.concatenate([one, two], axis=0)

    def scored(q, k):
        return lax.dot_general(q, k, (((1,), (1,)), ((), ())), preferred_element_type=F32)

    own = scored(two_maps(query), fresh_k)
    seen = jnp.concatenate([reach, reach], axis=0) > 0.5
    own = jnp.where(seen, own, -1e30)
    own_max = jnp.max(own, axis=1, keepdims=True)
    own_weights = jnp.exp(own - own_max)
    own_sums = jnp.sum(own_weights, axis=1, keepdims=True)
    own_weighted = dot(own_weights.astype(BF), fresh_v)
    eye = iota((pair, DV), 0) == iota((pair, DV), 1)

    def as_row(column):
        return jnp.sum(jnp.where(eye, column, 0.0), axis=0, keepdims=True)

    def as_column(row):
        return jnp.sum(jnp.where(eye, row, 0.0), axis=1, keepdims=True)

    own_max_row = as_row(own_max)
    own_sums_row = as_row(own_sums)

    shift = heads.bit_length() - 1
    valid = filled_ref[0] + accepted_ref[0]
    visible = me * span + iota((1, span), 1) < valid
    arrive(3, qg_recv)
    scores = jnp.concatenate([scored(two_maps(qg_recv[h]), kh[h]) for h in range(heads)], axis=0)
    scores = jnp.where(visible, scores, -1e30)
    highest = jnp.maximum(jnp.max(scores, axis=1, keepdims=True), -1e29)
    weights = jnp.exp(scores - highest)
    sums = jnp.sum(weights, axis=1, keepdims=True)
    weights = weights.astype(BF)
    top = iota((8, DV), 0) == 0
    for h in range(heads):
        part_of = slice(h * pair, (h + 1) * pair)
        u_send[h] = dot(weights[part_of], vh[h]).astype(UTYPE)
        ms_send[h] = jnp.where(top, as_row(highest[part_of]), as_row(sums[part_of]))
    spread(5, lambda peer: ms_send.at[peer], ms_recv)
    spread(6, lambda peer: u_send.at[peer], u_recv)
    ms_recv[me] = ms_send[me]
    u_recv[me] = u_send[me]

    arrive(4, kvg_recv)
    line = iota((count, DV), 0)
    relative = me * span + (line >> shift) - valid
    inside = (relative >= 0) & (relative < rows)
    target = (line & (heads - 1)) * rows + relative
    one_hot = jnp.where(inside & (target == iota((count, DV), 1)), 1.0, 0.0).astype(BF)
    all_k = jnp.concatenate([kvg_recv[h, :rows] for h in range(heads)], axis=0)
    all_v = jnp.concatenate([kvg_recv[h, rows:] for h in range(heads)], axis=0)
    ko[...] = jnp.where(inside, dot(one_hot, all_k), kc[...].astype(F32)).astype(BF)
    vo[...] = jnp.where(inside, dot(one_hot, all_v), vc[...].astype(F32)).astype(BF)
    arrive(5, ms_recv)
    peak = own_max_row
    for i in range(n):
        peak = jnp.maximum(peak, ms_recv[i, 0:1])
    factors = []
    own_factor = jnp.exp(own_max_row - peak)
    whole = own_sums_row * own_factor
    for i in range(n):
        factor = jnp.exp(ms_recv[i, 0:1] - peak)
        whole = whole + ms_recv[i, 1:2] * factor
        factors.append(factor)
    merged = own_weighted * as_column(own_factor / whole)
    shares = [as_column(factor / whole) for factor in factors]
    arrive(6, u_recv)
    for i in range(n):
        merged = merged + u_recv[i].astype(F32) * shares[i]
    head_out = merged[:rows] - scale_ref[me] * merged[rows:]
    spreadness = jnp.mean(head_out * head_out, axis=1, keepdims=True)
    head_out = (head_out * lax.rsqrt(spreadness + 1e-05) * hgain_ref[...]).astype(BF)
    hg_send[...] = head_out
    spread(7, lambda peer: hg_send, hg_recv)
    hg_recv[me] = head_out
    loads[8].wait()
    arrive(7, hg_recv)
    flat = jnp.concatenate([hg_recv[h] for h in range(heads)], axis=1)
    out = dot(flat, wo[...]).astype(BF)
    m_send[...] = out
    tcopies = []
    for peer in tpeers:
        copy = pltpu.make_async_remote_copy(
            src_ref=m_send,
            dst_ref=m_recv.at[tp],
            send_sem=tsend_sem.at[peer],
            recv_sem=trecv_sem.at[tp],
            device_id={"tp": peer},
            device_id_type=MESH,
        )
        copy.start()
        tcopies.append(copy)
    m_recv[tp] = out
    for copy in started:
        copy.wait_send()
    for peer in tpeers:
        pltpu.make_async_remote_copy(
            src_ref=m_recv.at[peer],
            dst_ref=m_recv.at[peer],
            send_sem=tsend_sem.at[peer],
            recv_sem=trecv_sem.at[peer],
            device_id={"tp": peer},
            device_id_type=MESH,
        ).wait_recv()
    mixed = m_recv[0].astype(F32)
    for i in range(1, n_tp):
        mixed = mixed + m_recv[i].astype(F32)
    mixed_ref[...] = mixed.astype(BF)
    for copy in tcopies:
        copy.wait_send()


def deliver(mixed, key, value, mixed_hbm, key_hbm, value_hbm, sem):
    copies = [
        pltpu.make_async_copy(src, dst, sem.at[i])
        for i, (src, dst) in enumerate(((key, key_hbm), (value, value_hbm), (mixed, mixed_hbm)))
    ]
    for copy in copies:
        copy.start()
    for copy in copies:
        copy.wait()


def fused(
    n,
    n_tp,
    tokens,
    norm_gain,
    query_weight,
    key_weight,
    value_weight,
    out_weight,
    diff_scale,
    head_gain,
    key_cache,
    value_cache,
    cache_filled,
    accepted,
    parents,
):
    rows, features = tokens.shape
    heads = key_cache.shape[2]
    count = key_cache.shape[1] * heads
    width = out_weight.shape[1]
    vmem = pl.BlockSpec(memory_space=pltpu.VMEM)
    smem = pl.BlockSpec(memory_space=pltpu.SMEM)
    hbm = pl.BlockSpec(memory_space=pltpu.HBM)
    cache_shape = pltpu.VMEM((count, DV), BF)
    kept = 2 * (rows * width + 2 * count * DV) + (1 << 14)
    mixed, key_out, value_out = pl.pallas_call(
        functools.partial(kernel, n, n_tp, heads),
        out_shape=(pltpu.VMEM((rows, width), BF), cache_shape, cache_shape),
        in_specs=[hbm] * 9 + [smem] * 4,
        out_specs=(vmem, vmem, vmem),
        scratch_shapes=[
            pltpu.VMEM(tokens.shape, BF),
            pltpu.VMEM((features // DV, DV), BF),
            pltpu.VMEM((1, DV), F32),
            pltpu.VMEM(query_weight.shape, BF),
            pltpu.VMEM(key_weight.shape, BF),
            pltpu.VMEM(value_weight.shape, BF),
            pltpu.VMEM(out_weight.shape, BF),
            pltpu.VMEM((count, DV), BF),
            pltpu.VMEM((count, DV), BF),
            pltpu.VMEM((count, DV), F32),
            pltpu.VMEM((count, DV), F32),
            pltpu.VMEM((heads, count // heads, DV), BF),
            pltpu.VMEM((heads, count // heads, DV), BF),
            pltpu.VMEM((rows, DV), F32),
            pltpu.VMEM((n, rows, DV), F32),
            pltpu.VMEM((heads, rows, DV), PART),
            pltpu.VMEM((n, rows, DV), PART),
            pltpu.VMEM((heads, 2 * rows, DV), PART),
            pltpu.VMEM((n, 2 * rows, DV), PART),
            pltpu.VMEM((rows, DV), BF),
            pltpu.VMEM((n, rows, DV), BF),
            pltpu.VMEM((2 * rows, DV), BF),
            pltpu.VMEM((n, 2 * rows, DV), BF),
            pltpu.VMEM((heads, 2 * rows, DV), UTYPE),
            pltpu.VMEM((n, 2 * rows, DV), UTYPE),
            pltpu.VMEM((heads, 8, DV), F32),
            pltpu.VMEM((n, 8, DV), F32),
            pltpu.VMEM((rows, DV), BF),
            pltpu.VMEM((n, rows, DV), BF),
            pltpu.VMEM((rows, width), BF),
            pltpu.VMEM((n_tp, rows, width), BF),
            pltpu.SemaphoreType.DMA((9,)),
            pltpu.SemaphoreType.DMA((8, n)),
            pltpu.SemaphoreType.DMA((8, n)),
            pltpu.SemaphoreType.DMA((n_tp,)),
            pltpu.SemaphoreType.DMA((n_tp,)),
        ],
        compiler_params=pltpu.CompilerParams(collective_id=0, has_side_effects=True, vmem_limit_bytes=VMEM_BYTES - kept),
    )(
        tokens,
        norm_gain.reshape(features // DV, DV),
        head_gain.reshape(1, DV),
        query_weight,
        key_weight,
        value_weight,
        out_weight,
        key_cache.reshape(count, DV),
        value_cache.reshape(count, DV),
        diff_scale,
        cache_filled,
        accepted,
        parents,
    )
    flat = [jax.ShapeDtypeStruct(out.shape, out.dtype) for out in (mixed, key_out, value_out)]
    mixed, key_out, value_out = pl.pallas_call(
        deliver,
        out_shape=flat,
        in_specs=[vmem] * 3,
        out_specs=[hbm] * 3,
        scratch_shapes=[pltpu.SemaphoreType.DMA((3,))],
        compiler_params=pltpu.CompilerParams(vmem_limit_bytes=4 << 20),
    )(mixed, key_out, value_out)
    return mixed, key_out.reshape(key_cache.shape), value_out.reshape(value_cache.shape)


def body(n, n_tp, *args):
    tokens, key_cache = args[0], args[8]
    seqs, heads = key_cache.shape[0], key_cache.shape[2]
    rows = tokens.shape[0]
    if seqs == 1 and heads == n and heads & (heads - 1) == 0 and rows % 16 == 0 and 2 * rows <= DV and tokens.shape[1] % DV == 0:
        return fused(n, n_tp, *args)
    return shards(*args)


def solution(mesh):
    in_specs = (
        P(None, "kv"),
        P("kv"),
        P("kv", "tp"),
        P("kv", "tp"),
        P("kv", "tp"),
        P("tp", "kv"),
        P("tp"),
        P(),
        P(None, "kv", "tp", None),
        P(None, "kv", "tp", None),
        P(),
        P(),
        P(),
    )
    out_specs = (P(None, "kv"), P(None, "kv", "tp", None), P(None, "kv", "tp", None))
    return jax.shard_map(
        functools.partial(body, mesh.shape["kv"], mesh.shape["tp"]), mesh=mesh, in_specs=in_specs, out_specs=out_specs, check_vma=False)
```

profile of v0, /device:TPU:0, one launch (start us, length us, event | category | flops | bytes accessed | tf_op | source)
XLA Modules:
  0.0 33.9 jit_solution(7788364050915268911)
XLA Ops:
  1.9 31.1 %shard_map.148 = (bf16[16,512]{1,0:T(8,128)(2,1)S(1)}, bf16[1024,128]{1,0:T(8,128)(2,1)S(1)}, bf16[1024,128]{1,0:T(8,128)(2,1)S(1)}) custom-call(bf16[16,512]{1,0:T(8,128)(2,1)} %tok_hbm.1, bf16[4,128]{1,0:T(4,128)(2,1)} %bitcast.8, f32[1,128]{1,0:T(1,128)} %bitcast.9, bf16[512,1024]{1,0:T(8,128)(2,1)} %wq_hbm.1, bf16[512,1024]{1,0:T(8,128)(2,1)} %wk_hbm.1, ...), custom_call_target="tpu_custom_call" | custom-call | tf_op jit(solution)/shard_map/pallas_call | solution.py:511
  33.1 0.8 %shard_map.149 = (bf16[16,512]{1,0:T(8,128)(2,1)}, bf16[1024,128]{1,0:T(8,128)(2,1)}, bf16[1024,128]{1,0:T(8,128)(2,1)}) custom-call(bf16[16,512]{1,0:T(8,128)(2,1)S(1)} %get-tuple-element.9.mixed, bf16[1024,128]{1,0:T(8,128)(2,1)S(1)} %get-tuple-element.10.key, bf16[1024,128]{1,0:T(8,128)(2,1)S(1)} %get-tuple-element.11.value), custom_call_target="tpu_custom_call" | custom-call | tf_op jit(solution)/shard_map/pallas_call | solution.py:571
where the time goes:
time: 34.1 us; the launch traced here: 33.9 us
  Pallas kernels  31.9 us (94%)
  between operations  1.93 us (6%)
    pallas_call x1, Pallas kernels, fused(): pl.pallas_call(functools.partial(kernel, n, n_tp, heads), out_shape=(pltp...  31.1 us
    pallas_call x1, Pallas kernels, fused(): pl.pallas_call(deliver, out_shape=flat, in_specs=[vmem] * 3, out_specs=[h...  0.82 us

commit v1 on v0

--- a/solution.py
+++ b/solution.py
@@ -180,10 +180,10 @@
     wo_hbm,
     kc_hbm,
     vc_hbm,
-    scale_ref,
-    filled_ref,
-    accepted_ref,
-    parents_ref,
+    scale_hbm,
+    filled_hbm,
+    accepted_hbm,
+    parents_hbm,
     mixed_ref,
     ko,
     vo,
@@ -218,6 +218,10 @@
     hg_recv,
     m_send,
     m_recv,
+    scale_ref,
+    filled_ref,
+    accepted_ref,
+    parents_ref,
     local_sem,
     send_sem,
     recv_sem,
@@ -240,6 +244,10 @@
             (vc_hbm, vc),
             (hgain_hbm, hgain_ref),
             (wo_hbm, wo),
+            (scale_hbm, scale_ref),
+            (filled_hbm, filled_ref),
+            (accepted_hbm, accepted_ref),
+            (parents_hbm, parents_ref),
         )
     ):
         load = pltpu.make_async_copy(src, dst, local_sem.at[i])
@@ -280,6 +288,8 @@
             ).wait_recv()
 
     loads[0].wait()
+    for i in range(9, 13):
+        loads[i].wait()
     loads[1].wait()
     xfloat = tok_ref[...].astype(F32)
     squares = jnp.sum(xfloat * xfloat, axis=1, keepdims=True)
@@ -511,7 +521,7 @@
     mixed, key_out, value_out = pl.pallas_call(
         functools.partial(kernel, n, n_tp, heads),
         out_shape=(pltpu.VMEM((rows, width), BF), cache_shape, cache_shape),
-        in_specs=[hbm] * 9 + [smem] * 4,
+        in_specs=[hbm] * 13,
         out_specs=(vmem, vmem, vmem),
         scratch_shapes=[
             pltpu.VMEM(tokens.shape, BF),
@@ -545,7 +555,11 @@
             pltpu.VMEM((n, rows, DV), BF),
             pltpu.VMEM((rows, width), BF),
             pltpu.VMEM((n_tp, rows, width), BF),
-            pltpu.SemaphoreType.DMA((9,)),
+            pltpu.SMEM((heads,), F32),
+            pltpu.SMEM((1,), jnp.int32),
+            pltpu.SMEM((1,), jnp.int32),
+            pltpu.SMEM(parents.shape, jnp.int32),
+            pltpu.SemaphoreType.DMA((13,)),
             pltpu.SemaphoreType.DMA((8, n)),
             pltpu.SemaphoreType.DMA((8, n)),
             pltpu.SemaphoreType.DMA((n_tp,)),

time: 34.1 us -> 33.5 us (0.982)
  Pallas kernels: 31.9 us -> 31.3 us
    pallas_call x1, Pallas kernels: 31.1 us -> 30.5 us  [fused(): pl.pallas_call(functools.partial(kernel, n, n_tp, heads), out_shape=(pltp...]
where the time goes in v1:
time: 33.5 us; the launch traced here: 33.3 us
  Pallas kernels  31.3 us (93%)
  between operations  1.93 us (6%)
    pallas_call x1, Pallas kernels, fused(): pl.pallas_call(functools.partial(kernel, n, n_tp, heads), out_shape=(pltp...  30.5 us
    pallas_call x1, Pallas kernels, fused(): pl.pallas_call(deliver, out_shape=flat, in_specs=[vmem] * 3, out_specs=[h...  0.82 us

profile of v1, /device:TPU:0, one launch (start us, length us, event | category | flops | bytes accessed | tf_op | source)
XLA Modules:
  0.0 33.3 jit_solution(6813349079825003706)
XLA Ops:
  1.9 30.5 %shard_map.148 = (bf16[16,512]{1,0:T(8,128)(2,1)S(1)}, bf16[1024,128]{1,0:T(8,128)(2,1)S(1)}, bf16[1024,128]{1,0:T(8,128)(2,1)S(1)}) custom-call(bf16[16,512]{1,0:T(8,128)(2,1)} %tok_hbm.1, bf16[4,128]{1,0:T(4,128)(2,1)} %bitcast.8, f32[1,128]{1,0:T(1,128)} %bitcast.9, bf16[512,1024]{1,0:T(8,128)(2,1)} %wq_hbm.1, bf16[512,1024]{1,0:T(8,128)(2,1)} %wk_hbm.1, ...), custom_call_target="tpu_custom_call" | custom-call | tf_op jit(solution)/shard_map/pallas_call | solution.py:521
  32.4 0.8 %shard_map.149 = (bf16[16,512]{1,0:T(8,128)(2,1)}, bf16[1024,128]{1,0:T(8,128)(2,1)}, bf16[1024,128]{1,0:T(8,128)(2,1)}) custom-call(bf16[16,512]{1,0:T(8,128)(2,1)S(1)} %get-tuple-element.9.mixed, bf16[1024,128]{1,0:T(8,128)(2,1)S(1)} %get-tuple-element.10.key, bf16[1024,128]{1,0:T(8,128)(2,1)S(1)} %get-tuple-element.11.value), custom_call_target="tpu_custom_call" | custom-call | tf_op jit(solution)/shard_map/pallas_call | solution.py:585
